TPU v7x, 32 devices: a whole 2x2x4 slice. The times are simulated.
32 devices in a mesh: ep: 4 (over y, x), tp: 8 (over z, core).
Axes of the slice: x: 2, y: 2, z: 4, core: 2. Of those that a mesh axis runs over, the one named last changes fastest.
Arguments:
- hidden_in: bfloat16 [128, 4096], P('ep'), may hold values from -6 to 6
- mix_gain: float32 [4096], replicated, may hold values from 0.1 to 1.9
- w_query: bfloat16 [4096, 2048], P('ep', 'tp'), may hold values from -0.09375 to 0.09375
- w_key: bfloat16 [4096, 2048], P('ep', 'tp'), may hold values from -0.09375 to 0.09375
- w_value: bfloat16 [4096, 2048], P('ep', 'tp'), may hold values from -0.09375 to 0.09375
- w_outgate: bfloat16 [4096, 2048], P('ep', 'tp'), may hold values from -0.09375 to 0.09375
- w_gates: bfloat16 [2, 4096, 32], P(None, None, 'tp'), may hold values from -0.09375 to 0.09375
- gate_bias: float32 [2, 32], P(None, 'tp'), may hold values from -1 to 4
- state_matrix: float32 [128, 32, 64, 64], P('ep', 'tp'), may hold values from -2 to 2
- state_norm: float32 [128, 32, 64], P('ep', 'tp'), may hold values from -2 to 2
- state_max: float32 [128, 32], P('ep', 'tp'), may hold values from -3 to 3
- w_mix_out: bfloat16 [2048, 4096], P('tp'), may hold values from -0.125 to 0.125
- ffn_gain: float32 [4096], replicated, may hold values from 0.1 to 1.9
- routes: int32 [128, 2], replicated, may hold values from 0 to 7, all different within a row; in each aligned block of 32 rows (0 to 31, 32 to 63, ...) at most 9 rows name the same one
- route_weights: float32 [128, 2], P('ep'), may hold values from 0.1 to 1
- expert_gate: bfloat16 [8, 4096, 2048], P('ep', None, 'tp'), may hold values from -0.09375 to 0.09375
- expert_up: bfloat16 [8, 4096, 2048], P('ep', None, 'tp'), may hold values from -0.09375 to 0.09375
- expert_down: bfloat16 [8, 2048, 4096], P('ep', 'tp'), may hold values from -0.125 to 0.125
- shared_gate: bfloat16 [4096, 1024], P(None, 'tp'), may hold values from -0.09375 to 0.09375
- shared_up: bfloat16 [4096, 1024], P(None, 'tp'), may hold values from -0.09375 to 0.09375
- shared_down: bfloat16 [1024, 4096], P('tp'), may hold values from -0.1875 to 0.1875
Outputs:
- result: bfloat16 [128, 4096], P('ep', 'tp')
- new_matrix: float32 [128, 32, 64, 64], P('ep', 'tp')
- new_norm: float32 [128, 32, 64], P('ep', 'tp')
- new_max: float32 [128, 32], P('ep', 'tp')
Inputs may be any that keep to these rules, and one draw needn't show every extreme that they name: `routes`: each row names 2 different experts. In each aligned block of 32 rows (the rows of one device group along ep) no expert is named by more than 9 rows, a bound that some block reaches.
All inputs are finite; a program needn't handle non-finite values.
Results may differ from a plain program's by a relative error of at most 0.023.
Values may be sent and summed in bfloat16 or wider, within the bound.
A program may use at most 64 MiB of HBM per device.

v0:
```python
import jax
import jax.numpy as jnp
from jax import lax
from jax.sharding import PartitionSpec as P

norm_eps = 1e-06


def rms_scale(inputs, scales):
    floats = inputs.astype(jnp.float32)
    return floats * lax.rsqrt(jnp.mean(floats * floats, -1, keepdims=True) + norm_eps) * scales


def slot_ranks(chosen, experts):
    flat_ids = chosen.reshape(-1)
    onehot = (flat_ids[:, None] == jnp.arange(experts, dtype=jnp.int32)[None, :]).astype(jnp.int32)
    earlier = jnp.cumsum(onehot, 0) - onehot
    return jnp.sum(earlier * onehot, 1).reshape(chosen.shape)


def per_device(
    hidden_in,
    mix_gain,
    w_query,
    w_key,
    w_value,
    w_outgate,
    w_gates,
    gate_bias,
    state_matrix,
    state_norm,
    state_max,
    w_mix_out,
    ffn_gain,
    routes,
    route_weights,
    expert_gate,
    expert_up,
    expert_down,
    shared_gate,
    shared_up,
    shared_down,
):
    ep_count = lax.axis_size("ep")
    tp_count = lax.axis_size("tp")
    group_index = lax.axis_index("ep")
    column_index = lax.axis_index("tp")
    seq_rows, width = hidden_in.shape
    heads_dev = state_matrix.shape[1]
    head_dim = state_matrix.shape[2]
    top_count = routes.shape[1]
    local_experts = expert_gate.shape[0]
    expert_total = local_experts * ep_count
    capacity = max(2, seq_rows * top_count // expert_total + 1)
    slot_count = ep_count * capacity
    slice_width = width // tp_count
    normed = rms_scale(hidden_in, mix_gain).astype(jnp.bfloat16)
    gathered = lax.all_to_all(normed, "ep", split_axis=1, concat_axis=0, tiled=True)
    joined = jnp.concatenate([w_query, w_key, w_value, w_outgate], 1)
    projected = lax.psum_scatter(
        jnp.dot(gathered, joined, preferred_element_type=jnp.float32).astype(jnp.bfloat16),
        "ep",
        scatter_dimension=0,
        tiled=True,
    )
    head_cols = heads_dev * head_dim

    def heads_of(role_index):
        part = projected[:, role_index * head_cols : (role_index + 1) * head_cols]
        return part.astype(jnp.float32).reshape(seq_rows, heads_dev, head_dim)

    query_heads = heads_of(0)
    key_heads = heads_of(1) * head_dim ** (-0.5)
    value_heads = heads_of(2)
    out_gate = heads_of(3)
    gate_pre = jnp.einsum("sd,gdh->gsh", normed, w_gates, preferred_element_type=jnp.float32)
    gate_pre = gate_pre + gate_bias[:, None, :]
    carried = jax.nn.log_sigmoid(gate_pre[1]) + state_max
    new_max = jnp.maximum(carried, gate_pre[0])
    forget_weight = jnp.exp(carried - new_max)[..., None]
    input_weight = jnp.exp(gate_pre[0] - new_max)[..., None]
    new_norm = forget_weight * state_norm + input_weight * key_heads
    new_matrix = (
        forget_weight[..., None] * state_matrix
        + (input_weight * value_heads)[..., :, None] * key_heads[..., None, :]
    )
    numerator = jnp.einsum(
        "shek,shk->she", new_matrix, query_heads, precision=lax.Precision.HIGHEST
    )
    denominator = jnp.maximum(jnp.abs(jnp.sum(new_norm * query_heads, -1)), 1.0)
    gated_out = (jax.nn.sigmoid(out_gate) * numerator / denominator[..., None]).reshape(
        seq_rows, head_cols
    )
    gated_out = gated_out.astype(jnp.bfloat16)
    mixed_part = jnp.dot(gated_out, w_mix_out, preferred_element_type=jnp.float32)
    mixed_own = lax.psum_scatter(
        mixed_part.astype(jnp.bfloat16), "tp", scatter_dimension=1, tiled=True
    ).astype(jnp.float32)
    residual_own = lax.dynamic_slice_in_dim(hidden_in, column_index * slice_width, slice_width, 1)
    stream_own = (residual_own.astype(jnp.float32) + mixed_own).astype(jnp.bfloat16)
    stream = lax.all_gather(stream_own, "tp", axis=1, tiled=True)
    ffn_in = rms_scale(stream, ffn_gain).astype(jnp.bfloat16)
    shared_hidden = (
        jax.nn.silu(jnp.dot(ffn_in, shared_gate, preferred_element_type=jnp.float32))
        * jnp.dot(ffn_in, shared_up, preferred_element_type=jnp.float32)
    ).astype(jnp.bfloat16)
    shared_part = jnp.dot(shared_hidden, shared_down, preferred_element_type=jnp.float32)
    own_routes = lax.dynamic_slice_in_dim(routes, group_index * seq_rows, seq_rows, 0)
    slot_ids = own_routes * capacity + slot_ranks(own_routes, expert_total)
    slot_range = jnp.arange(expert_total * capacity, dtype=jnp.int32)
    matches = slot_ids[:, :, None] == slot_range[None, None, :]
    chooser = jnp.any(matches, 1).astype(jnp.bfloat16)
    outgoing = jnp.einsum("sj,sd->jd", chooser, ffn_in, preferred_element_type=jnp.float32)
    outgoing = outgoing.astype(jnp.bfloat16).reshape(expert_total, capacity, width)
    arrived = lax.all_to_all(outgoing, "ep", split_axis=0, concat_axis=1, tiled=True)
    gate_values = jnp.einsum(
        "erd,edf->erf", arrived, expert_gate, preferred_element_type=jnp.float32
    )
    up_values = jnp.einsum("erd,edf->erf", arrived, expert_up, preferred_element_type=jnp.float32)
    expert_hidden = (jax.nn.silu(gate_values) * up_values).astype(jnp.bfloat16)
    expert_part = jnp.einsum(
        "erf,efd->erd", expert_hidden, expert_down, preferred_element_type=jnp.float32
    )
    expert_part = expert_part.reshape(local_experts * slot_count, width)
    routed_sum, shared_sum = (
        lax.psum_scatter(
            expert_part.astype(jnp.bfloat16), "tp", scatter_dimension=1, tiled=True
        ).astype(jnp.float32),
        lax.psum_scatter(
            shared_part.astype(jnp.bfloat16), "tp", scatter_dimension=1, tiled=True
        ).astype(jnp.float32),
    )
    expert_rows = routed_sum.astype(jnp.bfloat16)
    returned = lax.all_to_all(
        expert_rows.reshape(local_experts, slot_count, slice_width),
        "ep",
        split_axis=1,
        concat_axis=0,
        tiled=True,
    )
    returned = returned.reshape(expert_total * capacity, slice_width)
    weights = jnp.sum(jnp.where(matches, route_weights[:, :, None], 0.0), 1)
    routed = jnp.dot(weights, returned.astype(jnp.float32), precision=lax.Precision.HIGHEST)
    result = (stream_own.astype(jnp.float32) + shared_sum + routed).astype(jnp.bfloat16)
    return (result, new_matrix, new_norm, new_max)


def solution(mesh):
    placed = (
        P("ep", None),
        P(),
        P("ep", "tp"),
        P("ep", "tp"),
        P("ep", "tp"),
        P("ep", "tp"),
        P(None, None, "tp"),
        P(None, "tp"),
        P("ep", "tp", None, None),
        P("ep", "tp", None),
        P("ep", "tp"),
        P("tp", None),
        P(),
        P(),
        P("ep", None),
        P("ep", None, "tp"),
        P("ep", None, "tp"),
        P("ep", "tp", None),
        P(None, "tp"),
        P(None, "tp"),
        P("tp", None),
    )
    return jax.shard_map(
        per_device,
        mesh=mesh,
        in_specs=placed,
        out_specs=(P("ep", "tp"), P("ep", "tp", None, None), P("ep", "tp", None), P("ep", "tp")),
        check_vma=False,
    )
```

profile of v0, /device:TPU:0, one launch (start us, length us, event | category | flops | bytes accessed | tf_op | source)
XLA Modules:
  0.0 207.5 jit_solution(7990342096338553955)
XLA Ops:
  7.2 1.3 fusion.19
  8.4 1.1 fusion.21
  9.5 0.7 copy.88
  10.3 5.2 %all-to-all-start = ((bf16[32,4,1024]{2,0,1:T(8,128)(2,1)}), bf16[32,4,1024]{2,0,1:T(8,128)(2,1)S(1)}, u32[]{:S(2)}, u32[]{:S(2)}) async-start(bf16[32,4,1024]{2,0,1:T(8,128)(2,1)} %bitcast.53), calls=%async_computation | async-start | bytes 524288 | tf_op jit(solution)/shard_map/all_to_all | solution.py:58
  15.5 1.0 fusion.14
  16.5 4.3 %all-to-all-done = bf16[32,4,1024]{2,0,1:T(8,128)(2,1)S(1)} async-done(((bf16[32,4,1024]{2,0,1:T(8,128)(2,1)}), bf16[32,4,1024]{2,0,1:T(8,128)(2,1)S(1)}, u32[]{:S(2)}, u32[]{:S(2)}) %all-to-all-start) | async-done | bytes 262176 | tf_op jit(solution)/shard_map/all_to_all | solution.py:58
  20.8 2.7 %fusion.8 = bf16[128,1024]{1,0:T(8,128)(2,1)} fusion(bf16[128,1024]{1,0:T(8,128)(2,1)S(1)} %bitcast.60, bf16[1024,256]{1,0:T(8,128)(2,1)} %param.26, bf16[1024,256]{1,0:T(8,128)(2,1)} %param.25, bf16[1024,256]{1,0:T(8,128)(2,1)} %param.24, bf16[1024,256]{1,0:T(8,128)(2,1)} %param.23), kind=kOutput, calls=%fused_computation.13 | convolution fusion | flops 276955136 | bytes 2621440 | tf_op jit(solution)/shard_map/dot_general | solution.py:61
  24.2 23.9 %reduce-scatter.5.cloned.1.call-done = bf16[32,1024]{1,0:T(8,128)(2,1)} async-done(((bf16[128,1024]{1,0:T(8,128)(2,1)}), bf16[32,1024]{1,0:T(8,128)(2,1)}) %reduce-scatter.5.cloned.1.call-update) | async-done | bytes 65552 | tf_op jit(solution)/shard_map/reduce_scatter | solution.py:60
  48.1 0.8 fusion.54
  49.3 0.8 multiply_reduce_fusion
  50.1 0.7 add_divide_fusion
  50.9 3.7 %multiply_add_fusion = f32[32,4,64,64]{3,2,1,0:T(8,128)S(1)} fusion(f32[32,4,64,64]{3,2,1,0:T(8,128)} %param.29, f32[32,4,64]{2,1,0:T(4,128)S(1)} %get-tuple-element.9, f32[32,4,64]{2,1,0:T(4,128)S(1)} %get-tuple-element.13, f32[32,4]{1,0:T(8,128)S(1)} %copy.67), kind=kLoop, calls=%fused_computation.4 | loop fusion | flops 1572864 | bytes 4260352 | tf_op jit(solution)/shard_map/add | solution.py:84
  54.7 2.0 copy-done.1
  56.7 3.4 %fusion.55 = f32[32,4,1,64]{3,2,1,0:T(1,128)S(1)} fusion(f32[32,4,64,64]{3,2,1,0:T(8,128)S(1)} %multiply_add_fusion, bf16[32,4,64,1]{2,3,1,0:T(2,128)(2,1)S(1)} %reshape.111), kind=kOutput, calls=%fused_computation.85 | convolution fusion | flops 6291456 | bytes 2146304 | tf_op jit(solution)/shard_map/shek,shk->she/dot_general | solution.py:87
  60.3 1.2 convolution_convert_fusion.3
  62.1 30.2 %reduce-scatter.7.cloned.1.call-done = bf16[32,512]{1,0:T(8,128)(2,1)} async-done(((bf16[32,4096]{1,0:T(8,128)(2,1)}), bf16[32,512]{1,0:T(8,128)(2,1)}) %reduce-scatter.7.cloned.1.call-update) | async-done | bytes 32784 | tf_op jit(solution)/shard_map/reduce_scatter | solution.py:96
  92.3 0.8 add_convert_fusion
  93.1 14.2 %all_gather.3 = bf16[32,4096]{1,0:T(8,128)(2,1)S(1)} all-gather(bf16[32,512]{1,0:T(8,128)(2,1)S(1)} %add_convert_fusion), channel_id=1, replica_groups=mesh['ep'=4,'tp'=8] {'tp'}, dimensions={1}, use_global_device_ids=true | all-gather | bytes 294912 | tf_op jit(solution)/shard_map/all_gather | solution.py:101
  107.5 1.2 convolution_convert_fusion.1
  108.7 1.3 reshape.100
  110.0 18.2 %all_to_all.52 = bf16[8,9,4096]{2,1,0:T(8,128)(2,1)S(1)} all-to-all(bf16[8,9,4096]{2,1,0:T(8,128)(2,1)S(1)} %reshape.100), channel_id=1, replica_groups=mesh['ep'=4,'tp'=8] {'ep'}, dimensions={0} | all-to-all | bytes 1179648 | tf_op jit(solution)/shard_map/all_to_all | solution.py:115
  128.8 3.1 %fusion.17 = f32[2,36,256]{2,1,0:T(8,128)S(1)} fusion(bf16[2,4096,256]{2,1,0:T(8,128)(2,1)} %param.36, bf16[2,36,4096]{2,0,1:T(2,128)(2,1)S(1)} %bitcast.54), kind=kOutput, calls=%fused_computation.27 | convolution fusion | flops 150994944 | bytes 4857856 | tf_op jit(solution)/shard_map/erd,edf->erf/dot_general | solution.py:116
  131.9 6.0 %convolution_convert_fusion = bf16[2,36,4096]{2,1,0:T(8,128)(2,1)} fusion(bf16[2,256,4096]{2,1,0:T(8,128)(2,1)} %param.38, bf16[2,4096,256]{2,1,0:T(8,128)(2,1)} %param.37, bf16[2,36,4096]{2,0,1:T(2,128)(2,1)S(1)} %bitcast.55, f32[2,36,256]{2,1,0:T(8,128)S(1)} %fusion.17), kind=kOutput, calls=%fused_computation | convolution fusion | flops 302395392 | bytes 9641984 | tf_op jit(solution)/shard_map/erf,efd->erd/dot_general | solution.py:121
  137.9 2.0 convert_element_type.93
  140.0 1.6 fusion.51
  141.6 2.9 %convolution_convert_fusion.2 = bf16[32,4096]{1,0:T(8,128)(2,1)} fusion(bf16[128,4096]{1,0:T(8,128)(2,1)} %param.41, bf16[4096,128]{1,0:T(8,128)(2,1)} %param.40, f32[32,128]{1,0:T(8,128)S(1)} %fusion.51, bf16[32,4096]{1,0:T(8,128)(2,1)S(1)} %all_gather.3, f32[4096]{0:T(1024)S(1)} %copy-done.2, f32[32]{0:T(128)S(1)} %add_rsqrt_fusion), kind=kOutput, calls=%fused_computation.2 | convolution fusion | flops 67788800 | bytes 2654336 | tf_op jit(solution)/shard_map/dot_general | solution.py:107
  144.5 23.9 %reduce-scatter.11.cloned.1.call-done = bf16[72,512]{1,0:T(8,128)(2,1)} async-done(((bf16[72,4096]{1,0:T(8,128)(2,1)}), bf16[72,512]{1,0:T(8,128)(2,1)}) %reduce-scatter.11.cloned.1.call-update) | async-done | bytes 73744 | tf_op jit(solution)/shard_map/reduce_scatter | solution.py:126
  168.4 0.9 reshape.101
  170.0 3.6 %all-to-all-start.2 = ((bf16[2,36,512]{2,0,1:T(2,128)(2,1)}), bf16[2,36,512]{2,0,1:T(2,128)(2,1)S(1)}, u32[]{:S(2)}, u32[]{:S(2)}) async-start(bf16[2,36,512]{2,0,1:T(2,128)(2,1)} %copy.76), calls=%async_computation.6 | async-start | bytes 147456 | tf_op jit(solution)/shard_map/all_to_all | solution.py:134
  173.7 4.8 %all-to-all-done.2 = bf16[2,36,512]{2,0,1:T(2,128)(2,1)S(1)} async-done(((bf16[2,36,512]{2,0,1:T(2,128)(2,1)}), bf16[2,36,512]{2,0,1:T(2,128)(2,1)S(1)}, u32[]{:S(2)}, u32[]{:S(2)}) %all-to-all-start.2) | async-done | bytes 73760 | tf_op jit(solution)/shard_map/all_to_all | solution.py:134
  178.5 20.9 %reduce-scatter.9.cloned.1.call-done = bf16[32,512]{1,0:T(8,128)(2,1)} async-done(((bf16[32,4096]{1,0:T(8,128)(2,1)}), bf16[32,512]{1,0:T(8,128)(2,1)}) %reduce-scatter.9.cloned.1.call-update) | async-done | bytes 32784 | tf_op jit(solution)/shard_map/reduce_scatter | solution.py:129
  199.4 1.5 fusion.12
  (54 shorter events, 3.8 us)
Async XLA Ops:
  7.2 53.1 %copy-start = (bf16[256,4096]{1,0:T(8,128)(2,1)S(1)}, bf16[256,4096]{1,0:T(8,128)(2,1)}, u32[]{:S(2)}) copy-start(bf16[256,4096]{1,0:T(8,128)(2,1)} %param.32) | copy-start | bytes 6291460
  10.3 10.6 %all-to-all-start = ((bf16[32,4,1024]{2,0,1:T(8,128)(2,1)}), bf16[32,4,1024]{2,0,1:T(8,128)(2,1)S(1)}, u32[]{:S(2)}, u32[]{:S(2)}) async-start(bf16[32,4,1024]{2,0,1:T(8,128)(2,1)} %bitcast.53), calls=%async_computation | async-start | bytes 524288 | tf_op jit(solution)/shard_map/all_to_all | solution.py:58
  15.5 32.7 %reduce-scatter.5.cloned.1.call-start = ((), (), s32[]{:S(2)}) async-start(), calls=%async_computation.7 | async-start | bytes 327680 | tf_op jit(solution)/shard_map/reduce_scatter | solution.py:60
  16.5 7.1 %copy-start.4 = (f32[32,4]{0,1:T(4,128)S(1)}, f32[32,4]{0,1:T(4,128)}, u32[]{:S(2)}) copy-start(f32[32,4]{0,1:T(4,128)} %param.31) | copy-start | bytes 1540
  20.8 3.1 %copy-start.7 = (s32[128,2]{0,1:T(2,128)S(1)}, s32[128,2]{0,1:T(2,128)}, u32[]{:S(2)}) copy-start(s32[128,2]{0,1:T(2,128)} %param.34) | copy-start | bytes 3076
  20.8 28.4 %copy-start.3 = (f32[32,4,64]{2,1,0:T(4,128)S(1)}, f32[32,4,64]{2,1,0:T(4,128)}, u32[]{:S(2)}) copy-start(f32[32,4,64]{2,1,0:T(4,128)} %param.30) | copy-start | bytes 98308
  23.6 68.8 %reduce-scatter.7.cloned.1.call-start = ((), (), s32[]{:S(2)}) async-start(), calls=%async_computation.8 | async-start | bytes 294912 | tf_op jit(solution)/shard_map/reduce_scatter | solution.py:96
  23.6 31.0 %copy-start.5 = (f32[32,4]{0,1:T(4,128)}, f32[32,4]{0,1:T(4,128)S(1)}, u32[]{:S(2)}) copy-start(f32[32,4]{0,1:T(4,128)S(1)} %get-tuple-element.8) | copy-start | bytes 1540
  54.6 2.0 copy-start.1
  56.7 50.8 %copy-start.2 = (f32[4096]{0:T(1024)S(1)}, f32[4096]{0:T(1024)}, u32[]{:S(2)}) copy-start(f32[4096]{0:T(1024)} %param.33) | copy-start | bytes 49156
  61.4 106.9 %reduce-scatter.11.cloned.1.call-start = ((), (), s32[]{:S(2)}) async-start(), calls=%async_computation.10 | async-start | bytes 663552 | tf_op jit(solution)/shard_map/reduce_scatter | solution.py:126
  137.9 35.7 %copy-start.6 = (f32[32,2]{0,1:T(2,128)S(1)}, f32[32,2]{0,1:T(2,128)}, u32[]{:S(2)}) copy-start(f32[32,2]{0,1:T(2,128)} %param.35) | copy-start | bytes 772
  140.0 59.4 %reduce-scatter.9.cloned.1.call-start = ((), (), s32[]{:S(2)}) async-start(), calls=%async_computation.9 | async-start | bytes 294912 | tf_op jit(solution)/shard_map/reduce_scatter | solution.py:129
  170.0 8.5 %all-to-all-start.2 = ((bf16[2,36,512]{2,0,1:T(2,128)(2,1)}), bf16[2,36,512]{2,0,1:T(2,128)(2,1)S(1)}, u32[]{:S(2)}, u32[]{:S(2)}) async-start(bf16[2,36,512]{2,0,1:T(2,128)(2,1)} %copy.76), calls=%async_computation.6 | async-start | bytes 147456 | tf_op jit(solution)/shard_map/all_to_all | solution.py:134
Sparse Core Ops, SparseCore 0:
  23.7 24.3 reduce-scatter.4
  61.6 30.7 reduce-scatter.6
  140.1 28.2 reduce-scatter.10
  170.5 28.9 reduce-scatter.8
where the time goes:
time: 208 us
  waiting for transfers between devices  108 us (52%)
  blocking collectives  32.4 us (16%)
  matrix products  24.5 us (12%)
  between operations  14 us (7%)
  other arithmetic  10 us (5%)
  local copies, waits for them, and re-layouts  9.69 us (5%)
  starting transfers between devices  8.96 us (4%)
    reduce_scatter x1, waiting for transfers between devices, per_device(): lax.psum_scatter(mixed_part.astype(jnp.bfloat16), 'tp', scatter_dimension...  30.2 us
    reduce_scatter x1, waiting for transfers between devices, per_device(): lax.psum_scatter(jnp.dot(gathered, joined, preferred_element_type=jnp.flo...  23.9 us
    reduce_scatter x1, waiting for transfers between devices, per_device(): lax.psum_scatter(expert_part.astype(jnp.bfloat16), 'tp', scatter_dimensio...  23.9 us
    reduce_scatter x1, waiting for transfers between devices, per_device(): lax.psum_scatter(shared_part.astype(jnp.bfloat16), 'tp', scatter_dimensio...  20.9 us
    all_to_all x1, blocking collectives, per_device(): lax.all_to_all(outgoing, 'ep', split_axis=0, concat_axis=1, tiled=True)  18.2 us
    all_gather x1, blocking collectives, per_device(): stream = lax.all_gather(stream_own, 'tp', axis=1, tiled=True)  14.2 us
    dot_general x1, matrix products, per_device(): jnp.einsum('erf,efd->erd', expert_hidden, expert_down, preferred_element_...  6.02 us
    all_to_all x1, starting transfers between devices, per_device(): lax.all_to_all(normed, 'ep', split_axis=1, concat_axis=0, tiled=True)  5.19 us
  transfers between devices with their start and end apart: 6, of which 6 were waited for; matrix products, arithmetic and copies ran while one was open for 4% of the time, Pallas kernels for 0%

commit v1 on v0

v1 whole, which is shorter than its diff:
```python
import functools

import jax
import jax.numpy as jnp
from jax import lax
from jax.experimental import pallas as pl
from jax.experimental.pallas import tpu as pltpu
from jax.sharding import PartitionSpec as P

norm_eps = 1e-06
F32 = jnp.float32
BF16 = jnp.bfloat16
MESH = pl.DeviceIdType.MESH


def dot(a, b):
    return jnp.dot(a, b, preferred_element_type=F32)


def layer_kernel(
    dims,
    hidden_ref,
    mix_gain_ref,
    w_gates_ref,
    bias_ref,
    norm_ref,
    max_ref,
    ffn_gain_ref,
    routes_ref,
    weights_ref,
    wq_hbm,
    wk_hbm,
    wv_hbm,
    wo_hbm,
    state_hbm,
    mix_hbm,
    sg_hbm,
    su_hbm,
    sd_hbm,
    eg_hbm,
    eu_hbm,
    ed_hbm,
    result_ref,
    new_max_ref,
    new_norm_ref,
    forget_ref,
    iv_ref,
    kk_ref,
    wq,
    wk,
    wv,
    wo,
    state,
    mix,
    sg,
    su,
    sd,
    eg,
    eu,
    ed,
    normed,
    gathered,
    part,
    proj_in,
    q_heads,
    pads,
    routes_t,
    mix_out,
    mix_in,
    mix_own,
    zs,
    zr,
    half,
    other,
    sel,
    rx_a,
    rx_b,
    x_shared,
    sh_out,
    sh_in,
    sh_own,
    x_rows,
    hid,
    pair_out,
    pair_in,
    pair_own,
    ret_out,
    ret_in,
    comb,
    zs2,
    zr2,
    local_sem,
    send_sem,
    recv_sem,
):
    E, T, S, D, H, hd, Le, cap, pad_rows, top = dims
    Z = T // 2
    SW = D // T
    Dk = D // E
    rows = Le * cap
    g = lax.axis_index("ep")
    t = lax.axis_index("tp")
    z = lax.div(t, 2)
    c = lax.rem(t, 2)
    partner = {"tp": t + 1 - 2 * c}
    locals_ = []
    for n, (src, dst) in enumerate(
        zip(
            (wq_hbm, wk_hbm, wv_hbm, wo_hbm, state_hbm, mix_hbm, sg_hbm, su_hbm, sd_hbm, eg_hbm, eu_hbm, ed_hbm),
            (wq, wk, wv, wo, state, mix, sg, su, sd, eg, eu, ed),
        )
    ):
        copy = pltpu.make_async_copy(src, dst, local_sem.at[n])
        copy.start()
        locals_.append(copy)

    barrier = pltpu.get_barrier_semaphore()
    lo = rows // 16 * 16
    if lo < pad_rows:
        for buf in (rx_a, rx_b, ret_in):
            buf[:, lo:, :] = jnp.zeros((E, pad_rows - lo, Z * SW), BF16)
    pl.semaphore_signal(barrier, inc=1, device_id=partner, device_id_type=MESH)
    for d in range(1, Z):
        pl.semaphore_signal(barrier, inc=1, device_id={"tp": lax.rem(z + d, Z) * 2 + c}, device_id_type=MESH)
    for d in range(1, E):
        pl.semaphore_signal(barrier, inc=1, device_id={"ep": lax.rem(g + d, E)}, device_id_type=MESH)

    sent = []

    def remote(src, dst, device):
        n = len(sent)
        copy = pltpu.make_async_remote_copy(
            src_ref=src,
            dst_ref=dst,
            send_sem=send_sem.at[n],
            recv_sem=recv_sem.at[n],
            device_id=device,
            device_id_type=MESH,
        )
        copy.start()
        sent.append(copy)
        return copy

    def ep_to(d):
        return lax.rem(g + d, E)

    def ep_from(d):
        return lax.rem(g + E - d, E)

    def z_to(d):
        return lax.rem(z + d, Z)

    def z_from(d):
        return lax.rem(z + Z - d, Z)

    def columns(zi, core):
        return pl.ds(pl.multiple_of((zi * 2 + core) * SW, SW), SW)

    def transposed(slot, value):
        pads[slot] = jnp.zeros((8, 128), F32)
        pads[slot, : value.shape[0], : value.shape[1]] = value
        return pads[slot].T

    floats = hidden_ref[...].astype(F32)
    scale = lax.rsqrt(jnp.mean(floats * floats, -1, keepdims=True) + norm_eps)
    for p in range(E):
        span = slice(p * Dk, (p + 1) * Dk)
        normed[p] = (hidden_ref[:, span].astype(F32) * scale * mix_gain_ref[:, span]).astype(BF16)
    pl.semaphore_wait(barrier, Z + E - 1)
    moves = [remote(normed.at[ep_to(d)], gathered.at[g], {"ep": ep_to(d)}) for d in range(1, E)]
    gathered[g] = normed[g]

    bias_t = transposed(0, bias_ref[...])
    gate_pre = []
    for role in range(2):
        total = jnp.zeros((H, S), F32)
        for p in range(E):
            total = total + lax.dot_general(
                w_gates_ref[role, :, p * Dk : (p + 1) * Dk],
                normed[p],
                (((1,), (1,)), ((), ())),
                preferred_element_type=F32,
            )
        gate_pre.append(total + bias_t[:H, role : role + 1])
    carried = jnp.minimum(gate_pre[1], 0.0) - jnp.log(1.0 + jnp.exp(-jnp.abs(gate_pre[1]))) + max_ref[...]
    new_max = jnp.maximum(carried, gate_pre[0])
    forget = jnp.exp(carried - new_max)
    take = jnp.exp(gate_pre[0] - new_max)
    new_max_ref[...] = new_max
    forget_ref[...] = forget
    forget_t = transposed(1, forget)
    take_t = transposed(2, take)

    route_floats = routes_ref[...].astype(F32)
    routes_t[...] = jnp.concatenate(
        [route_floats, jnp.zeros((8 - top, route_floats.shape[1]), F32)], 0
    ).T
    own_routes = routes_t[pl.ds(pl.multiple_of(g * S, 8), S), :]
    weights_t = transposed(3, weights_ref[...])
    lane = lax.broadcasted_iota(jnp.int32, (S, 128), 1).astype(F32)
    named = [(own_routes[:, k : k + 1] == lane).astype(F32) for k in range(top)]
    onehot = functools.reduce(jnp.add, named)
    earlier = (
        lax.broadcasted_iota(jnp.int32, (S, S), 0) > lax.broadcasted_iota(jnp.int32, (S, S), 1)
    ).astype(F32)
    rank = dot(earlier.astype(BF16), onehot.astype(BF16))
    owner = jnp.floor((lane + 0.5) / Le)
    base = rank + owner * pad_rows + (lane - owner * Le) * cap
    slot_lane = lax.broadcasted_iota(jnp.int32, (S, E * pad_rows), 1).astype(F32)
    match = jnp.zeros((S, E * pad_rows), F32)
    share = jnp.zeros((S, E * pad_rows), F32)
    for k in range(top):
        slot = jnp.sum(base * named[k], -1, keepdims=True)
        hit = slot_lane == slot
        match = jnp.where(hit, 1.0, match)
        share = jnp.where(hit, weights_t[:S, k : k + 1], share)
    chooser = match.T.astype(BF16)
    share_hi = share.astype(BF16)
    share_lo = (share - share_hi.astype(F32)).astype(BF16)

    for n in range(4):
        locals_[n].wait()
    for move in moves:
        move.wait_recv()
    stacked = gathered[...].reshape(E * S, Dk)
    hc = H * hd
    for n, weight in enumerate((wq, wk, wv, wo)):
        part[:, :, n * hc : (n + 1) * hc] = dot(stacked, weight[...]).astype(BF16).reshape(E, S, hc)
    moves = [remote(part.at[ep_to(d)], proj_in.at[g], {"ep": ep_to(d)}) for d in range(1, E)]
    locals_[4].wait()
    for move in moves:
        move.wait_recv()
    projected = part[g].astype(F32)
    for d in range(1, E):
        projected = projected + proj_in[ep_from(d)].astype(F32)
    projected = projected.astype(BF16).astype(F32)

    for h in range(H):
        q_heads[h] = projected[:, h * hd : (h + 1) * hd]
    lane64 = lax.broadcasted_iota(jnp.int32, (hd, 128), 1)

    def read_row(s, totals):
        out = []
        for h in range(H):
            product = state[s, h] * q_heads[h, pl.ds(s, 1), :]
            out.append(jnp.where(lane64 == s, jnp.sum(product, -1, keepdims=True), totals[h]))
        return tuple(out)

    reads = lax.fori_loop(0, S, read_row, tuple(jnp.zeros((hd, 128), F32) for _ in range(H)))
    gated = []
    for h in range(H):
        query = q_heads[h]
        key = projected[:, hc + h * hd : hc + (h + 1) * hd] * hd ** (-0.5)
        value = projected[:, 2 * hc + h * hd : 2 * hc + (h + 1) * hd]
        gate = projected[:, 3 * hc + h * hd : 3 * hc + (h + 1) * hd]
        keep = forget_t[:S, h : h + 1]
        put = take_t[:S, h : h + 1]
        put_value = put * value
        new_norm = keep * norm_ref[:, h, :] + put * key
        new_norm_ref[:, h, :] = new_norm
        iv_ref[:, h, :] = put_value
        kk_ref[:, h, :] = key
        numerator = keep * reads[h].T[:S, :] + put_value * jnp.sum(key * query, -1, keepdims=True)
        denominator = jnp.maximum(jnp.abs(jnp.sum(new_norm * query, -1, keepdims=True)), 1.0)
        gated.append(numerator / (denominator * (1.0 + jnp.exp(-gate))))
    gated = jnp.concatenate(gated, -1).astype(BF16)

    locals_[5].wait()
    moves = []
    for zi in range(Z):
        mix_out[zi] = dot(gated, mix[:, columns(zi, 1 - c)]).astype(BF16)
        moves.append(remote(mix_out.at[zi], mix_in.at[zi], partner))
    for zi in range(Z):
        mix_own[zi] = dot(gated, mix[:, columns(zi, c)])
    for move in moves:
        move.wait_recv()
    moves = []
    for d in range(1, Z):
        to = z_to(d)
        zs[to] = (mix_own[to] + mix_in[to].astype(F32)).astype(BF16)
        moves.append(remote(zs.at[to], zr.at[z], {"tp": to * 2 + c}))
    mixed = hidden_ref[:, columns(z, c)].astype(F32) + mix_own[z] + mix_in[z].astype(F32)
    for d in range(1, Z):
        moves[d - 1].wait_recv()
        mixed = mixed + zr[z_from(d)].astype(F32)
    stream_own = mixed.astype(BF16)

    half[z] = stream_own
    moves = [remote(half.at[z], half.at[z], {"tp": z_to(d) * 2 + c}) for d in range(1, Z)]
    shares = [remote(half.at[z], other.at[z], partner)]
    for d in range(1, Z):
        moves[d - 1].wait_recv()
        shares.append(remote(half.at[z_from(d)], other.at[z_from(d)], partner))
    for zi in range(Z):
        sel[:, :, zi * SW : (zi + 1) * SW] = dot(chooser, half[zi]).astype(BF16).reshape(E, pad_rows, SW)
    kept = pl.ds(0, -(-rows // 8) * 8)
    moves = [
        remote(sel.at[ep_to(d), kept], rx_a.at[g, kept], {"ep": ep_to(d)}) for d in range(1, E)
    ]
    rows_shares = [remote(sel.at[g, kept], rx_b.at[g, kept], partner)]
    rx_a[g] = sel[g]

    for move in shares:
        move.wait_recv()
    squares = jnp.zeros((S, 1), F32)
    for zi in range(Z):
        for buf in (half, other):
            floats = buf[zi].astype(F32)
            squares = squares + jnp.sum(floats * floats, -1, keepdims=True)
    scale = lax.rsqrt(squares / D + norm_eps)
    for zi in range(Z):
        for buf, core in ((half, c), (other, 1 - c)):
            span = columns(zi, core)
            x_shared[:, span] = (buf[zi].astype(F32) * scale * ffn_gain_ref[:, span]).astype(BF16)
    for n in range(6, 9):
        locals_[n].wait()
    inputs = x_shared[...]
    gate = dot(inputs, sg[...])
    shared_hidden = (gate / (1.0 + jnp.exp(-gate)) * dot(inputs, su[...])).astype(BF16)
    shared_moves = []
    for zi in range(Z):
        sh_out[zi] = dot(shared_hidden, sd[:, columns(zi, 1 - c)]).astype(BF16)
        shared_moves.append(remote(sh_out.at[zi], sh_in.at[zi], partner))
    for zi in range(Z):
        sh_own[zi] = dot(shared_hidden, sd[:, columns(zi, c)])

    for d in range(1, E):
        moves[d - 1].wait_recv()
        rows_shares.append(remote(rx_a.at[ep_from(d), kept], rx_b.at[ep_from(d), kept], partner))
    for move in rows_shares:
        move.wait_recv()
    count = E * pad_rows
    squares = jnp.zeros((count, 1), F32)
    for buf in (rx_a, rx_b):
        for zi in range(Z):
            floats = buf[:, :, zi * SW : (zi + 1) * SW].reshape(count, SW).astype(F32)
            squares = squares + jnp.sum(floats * floats, -1, keepdims=True)
    scale = lax.rsqrt(squares / D + norm_eps)
    for zi in range(Z):
        for buf, core in ((rx_a, c), (rx_b, 1 - c)):
            span = columns(zi, core)
            floats = buf[:, :, zi * SW : (zi + 1) * SW].reshape(count, SW).astype(F32)
            x_rows[:, span] = (floats * scale * ffn_gain_ref[:, span]).astype(BF16)
    for n in range(9, 12):
        locals_[n].wait()
    width = eg.shape[2]
    place = lax.broadcasted_iota(jnp.int32, (E, pad_rows, width), 1).reshape(count, width)
    for e in range(Le):
        gate = dot(x_rows[...], eg[e])
        value = gate / (1.0 + jnp.exp(-gate)) * dot(x_rows[...], eu[e])
        value = jnp.where((place >= e * cap) & (place < (e + 1) * cap), value, 0.0)
        hid[:, e * width : (e + 1) * width] = value.astype(BF16)
    pair_moves = []
    for zi in range(Z):
        pair_out[zi] = dot(hid[...], ed[:, columns(zi, 1 - c)]).astype(BF16)
        pair_moves.append(remote(pair_out.at[zi], pair_in.at[zi], partner))
    for zi in range(Z):
        pair_own[zi] = dot(hid[...], ed[:, columns(zi, c)])
    for zi in range(Z):
        pair_moves[zi].wait_recv()
        both = pair_own[zi] + pair_in[zi].astype(F32)
        ret_out[:, :, zi * SW : (zi + 1) * SW] = both.astype(BF16).reshape(E, pad_rows, SW)
    moves = [
        remote(ret_out.at[ep_to(d), kept], ret_in.at[g, kept], {"ep": ep_to(d)})
        for d in range(1, E)
    ]
    ret_in[g] = ret_out[g]
    for move in shared_moves:
        move.wait_recv()
    for move in moves:
        move.wait_recv()

    for zi in range(Z):
        back = ret_in[:, :, zi * SW : (zi + 1) * SW].reshape(count, SW)
        comb[zi] = dot(share_hi, back) + dot(share_lo, back) + sh_own[zi] + sh_in[zi].astype(F32)
    moves = []
    for d in range(1, Z):
        to = z_to(d)
        zs2[to] = comb[to].astype(BF16)
        moves.append(remote(zs2.at[to], zr2.at[z], {"tp": to * 2 + c}))
    total = half[z].astype(F32) + comb[z]
    for d in range(1, Z):
        moves[d - 1].wait_recv()
        total = total + zr2[z_from(d)].astype(F32)
    result_ref[...] = total.astype(BF16)
    for copy in sent:
        copy.wait_send()


def per_device(
    hidden_in,
    mix_gain,
    w_query,
    w_key,
    w_value,
    w_outgate,
    w_gates,
    gate_bias,
    state_matrix,
    state_norm,
    state_max,
    w_mix_out,
    ffn_gain,
    routes,
    route_weights,
    expert_gate,
    expert_up,
    expert_down,
    shared_gate,
    shared_up,
    shared_down,
):
    E = lax.axis_size("ep")
    T = lax.axis_size("tp")
    S, D = hidden_in.shape
    H, hd = state_matrix.shape[1:3]
    top = routes.shape[1]
    Le, _, width = expert_gate.shape
    cap = max(2, S * top // (Le * E) + 1)
    pad_rows = -(-Le * cap // 16) * 16
    Z, SW, Dk, count = T // 2, D // T, D // E, E * pad_rows
    batch = routes.shape[0]
    dims = (E, T, S, D, H, hd, Le, cap, pad_rows, top)
    vmem = pl.BlockSpec(memory_space=pltpu.VMEM)
    hbm = pl.BlockSpec(memory_space=pl.ANY)
    down = expert_down.reshape(Le * width, D)
    big = (
        w_query, w_key, w_value, w_outgate, state_matrix, w_mix_out,
        shared_gate, shared_up, shared_down, expert_gate, expert_up, down,
    )
    V = pltpu.VMEM
    sems = 6 * E + 8 * Z + 8
    result, new_max, new_norm, forget, iv, kk = pl.pallas_call(
        functools.partial(layer_kernel, dims),
        out_shape=(
            jax.ShapeDtypeStruct((S, SW), BF16),
            jax.ShapeDtypeStruct((H, S), F32),
            jax.ShapeDtypeStruct((S, H, hd), F32),
            jax.ShapeDtypeStruct((H, S), F32),
            jax.ShapeDtypeStruct((S, H, hd), F32),
            jax.ShapeDtypeStruct((S, H, hd), F32),
        ),
        in_specs=[vmem] * 9 + [hbm] * len(big),
        out_specs=(vmem,) * 6,
        scratch_shapes=[V(a.shape, a.dtype) for a in big]
        + [
            V((E, S, Dk), BF16),
            V((E, S, Dk), BF16),
            V((E, S, 4 * H * hd), BF16),
            V((E, S, 4 * H * hd), BF16),
            V((H, S, hd), F32),
            V((4, 8, 128), F32),
            V((batch, 8), F32),
            V((Z, S, SW), BF16),
            V((Z, S, SW), BF16),
            V((Z, S, SW), F32),
            V((Z, S, SW), BF16),
            V((Z, S, SW), BF16),
            V((Z, S, SW), BF16),
            V((Z, S, SW), BF16),
            V((E, pad_rows, Z * SW), BF16),
            V((E, pad_rows, Z * SW), BF16),
            V((E, pad_rows, Z * SW), BF16),
            V((S, D), BF16),
            V((Z, S, SW), BF16),
            V((Z, S, SW), BF16),
            V((Z, S, SW), F32),
            V((count, D), BF16),
            V((count, Le * width), BF16),
            V((Z, count, SW), BF16),
            V((Z, count, SW), BF16),
            V((Z, count, SW), F32),
            V((E, pad_rows, Z * SW), BF16),
            V((E, pad_rows, Z * SW), BF16),
            V((Z, S, SW), F32),
            V((Z, S, SW), BF16),
            V((Z, S, SW), BF16),
            pltpu.SemaphoreType.DMA((len(big),)),
            pltpu.SemaphoreType.DMA((sems,)),
            pltpu.SemaphoreType.DMA((sems,)),
        ],
        compiler_params=pltpu.CompilerParams(
            collective_id=0, has_side_effects=True, vmem_limit_bytes=60 * 1024 * 1024
        ),
        name="layer",
    )(
        hidden_in,
        mix_gain.reshape(1, D),
        jnp.transpose(w_gates, (0, 2, 1)),
        gate_bias,
        state_norm,
        state_max.T,
        ffn_gain.reshape(1, D),
        routes.T,
        route_weights.T,
        *big,
    )
    new_matrix = forget.T[:, :, None, None] * state_matrix + iv[..., :, None] * kk[..., None, :]
    return (result, new_matrix, new_norm, new_max.T)


def solution(mesh):
    placed = (
        P("ep", None),
        P(),
        P("ep", "tp"),
        P("ep", "tp"),
        P("ep", "tp"),
        P("ep", "tp"),
        P(None, None, "tp"),
        P(None, "tp"),
        P("ep", "tp", None, None),
        P("ep", "tp", None),
        P("ep", "tp"),
        P("tp", None),
        P(),
        P(),
        P("ep", None),
        P("ep", None, "tp"),
        P("ep", None, "tp"),
        P("ep", "tp", None),
        P(None, "tp"),
        P(None, "tp"),
        P("tp", None),
    )
    return jax.shard_map(
        per_device,
        mesh=mesh,
        in_specs=placed,
        out_specs=(P("ep", "tp"), P("ep", "tp", None, None), P("ep", "tp", None), P("ep", "tp")),
        check_vma=False,
    )
```

time: 208 us -> 63.7 us (0.31)
  waiting for transfers between devices: 108 us -> 0 us
  Pallas kernels: 0 us -> 54.4 us
  blocking collectives: 32.4 us -> 0 us
  matrix products: 24.5 us -> 0 us
  between operations: 14 us -> 0.65 us
  starting transfers between devices: 8.96 us -> 0 us
  local copies, waits for them, and re-layouts: 9.69 us -> 2.59 us
  other arithmetic: 10 us -> 5.84 us
    reduce_scatter x4 -> x0, waiting for transfers between devices: 98.8 us -> none  [the longest x1 30.2 us: per_device(): lax.psum_scatter(mixed_part.astype(jnp.bfloat16), 'tp', scatter_dimension...]
    pallas_call x0 -> x1, Pallas kernels: none -> 54.4 us  [per_device(): pl.pallas_call(functools.partial(layer_kernel, dims), out_shape=(jax.Shap...]
    dot_general x10 -> x0, matrix products: 24.5 us -> none  [the longest x1 6.02 us: per_device(): jnp.einsum('erf,efd->erd', expert_hidden, expert_down, preferred_element_...]
    all_to_all x1 -> x0, blocking collectives: 18.2 us -> none  [per_device(): lax.all_to_all(outgoing, 'ep', split_axis=0, concat_axis=1, tiled=True)]
    all_gather x1 -> x0, blocking collectives: 14.2 us -> none  [per_device(): stream = lax.all_gather(stream_own, 'tp', axis=1, tiled=True)]
    all_to_all x2 -> x0, waiting for transfers between devices: 9.1 us -> none  [the longest x1 4.78 us: per_device(): lax.all_to_all(expert_rows.reshape(local_experts, slot_count, slice_width...]
    all_to_all x2 -> x0, starting transfers between devices: 8.83 us -> none  [the longest x1 5.19 us: per_device(): lax.all_to_all(normed, 'ep', split_axis=1, concat_axis=0, tiled=True)]
    reshape x9 -> x0, local copies, waits for them, and re-layouts: 3.41 us -> none  [the longest x2 1.58 us: per_device(): expert_rows.reshape(local_experts, slot_count, slice_width)]
  transfers between devices with their start and end apart: 6 -> 0, of which waited for: 6 -> 0; matrix products, arithmetic and copies ran while one was open for 4% -> 0% of each run, Pallas kernels for 0% -> 0%
where the time goes in v1:
time: 63.7 us; the launch traced here: 63.5 us
  Pallas kernels  54.4 us (85%)
  other arithmetic  5.84 us (9%)
  local copies, waits for them, and re-layouts  2.59 us (4%)
  between operations  0.65 us (1%)
    pallas_call x1, Pallas kernels, per_device(): pl.pallas_call(functools.partial(layer_kernel, dims), out_shape=(jax.Shap...  54.4 us
    add x1, other arithmetic, per_device(): forget.T[:, :, None, None] * state_matrix  5.84 us
    unnamed x9, local copies, waits for them, and re-layouts  1.83 us

profile of v1, /device:TPU:0, one launch (start us, length us, event | category | flops | bytes accessed | tf_op | source)
XLA Modules:
  0.0 63.5 jit_solution(10273432208967820592)
XLA Ops:
  0.6 54.4 %layer.1 = (bf16[32,512]{1,0:T(8,128)(2,1)}, f32[4,32]{1,0:T(4,128)}, f32[32,4,64]{2,1,0:T(4,128)}, f32[4,32]{1,0:T(4,128)}, f32[32,4,64]{2,1,0:T(4,128)}, /*index=5*/f32[32,4,64]{2,1,0:T(4,128)}) custom-call(bf16[32,4096]{1,0:T(8,128)(2,1)} %hidden_ref.1, f32[1,4096]{1,0:T(1,128)} %bitcast.11, bf16[2,4,4096]{2,1,0:T(4,128)(2,1)} %bitcast.10, ...), custom_call_target="tpu_custom_call" | custom-call | tf_op jit(solution)/shard_map/layer/pallas_call | solution.py:433
  55.0 0.8 %copy.25 = f32[32,4]{1,0:T(8,128)S(1)} copy(f32[32,4]{0,1:T(4,128)} %bitcast.13) | data formatting | bytes 1024 | tf_op jit(solution)/shard_map/transpose | solution.py:498
  55.8 0.0 copy-start.1
  55.8 0.0 copy-start
  55.8 0.0 copy-start.2
  55.8 5.8 %multiply_add_fusion = f32[32,4,64,64]{3,2,1,0:T(8,128)} fusion(f32[32,4,64,64]{3,2,1,0:T(8,128)} %state_hbm.1, f32[32,4,64]{2,1,0:T(4,128)} %get-tuple-element.13, f32[32,4,64]{2,1,0:T(4,128)} %get-tuple-element.12, f32[32,4]{1,0:T(8,128)S(1)} %copy.25), kind=kLoop, calls=%fused_computation | loop fusion | flops 1572864 | bytes 4260352 | tf_op jit(solution)/shard_map/add | solution.py:498
  61.6 0.0 copy-done.1
  61.6 0.6 copy.29
  62.2 0.0 copy-done
  62.2 0.6 copy.30
  62.9 0.0 copy-done.2
  62.9 0.6 copy.31
Async XLA Ops:
  55.8 5.9 %copy-start.1 = (bf16[32,512]{1,0:T(8,128)(2,1)S(1)}, bf16[32,512]{1,0:T(8,128)(2,1)}, u32[]{:S(2)}) copy-start(bf16[32,512]{1,0:T(8,128)(2,1)} %get-tuple-element.20) | copy-start | bytes 98308
  55.8 6.5 %copy-start = (f32[32,4,64]{2,1,0:T(4,128)S(1)}, f32[32,4,64]{2,1,0:T(4,128)}, u32[]{:S(2)}) copy-start(f32[32,4,64]{2,1,0:T(4,128)} %get-tuple-element.22) | copy-start | bytes 98308
  55.8 7.1 %copy-start.2 = (f32[4,32]{1,0:T(4,128)S(1)}, f32[4,32]{1,0:T(4,128)}, u32[]{:S(2)}) copy-start(f32[4,32]{1,0:T(4,128)} %get-tuple-element.15) | copy-start | bytes 1540

commit v2 on v1

--- a/solution.py
+++ b/solution.py
@@ -15,6 +15,46 @@
 
 def dot(a, b):
     return jnp.dot(a, b, preferred_element_type=F32)
+
+
+def flipped(index, mask):
+    out, bit = index, 1
+    while bit <= mask:
+        if mask & bit:
+            out = out + bit * (1 - 2 * lax.rem(lax.div(index, bit), 2))
+        bit *= 2
+    return out
+
+
+def partners(index, count):
+    if count & (count - 1) == 0:
+        return [(flipped(index, m), flipped(index, m)) for m in range(1, count)]
+    return [(lax.rem(index + d, count), lax.rem(index + count - d, count)) for d in range(1, count)]
+
+
+def memory_kernel(
+    result_in, norm_in, max_in, forget, iv, kk, state_hbm, result, matrix_hbm, norm, new_max,
+    state, matrix, in_sem, out_sem,
+):
+    pieces, size, heads = state.shape[:3]
+    ins, outs = [], []
+    for n in range(pieces):
+        span = pl.ds(n * size, size)
+        ins.append(pltpu.make_async_copy(state_hbm.at[span], state.at[n], in_sem.at[n]))
+        outs.append(pltpu.make_async_copy(matrix.at[n], matrix_hbm.at[span], out_sem.at[n]))
+        ins[n].start()
+    result[...] = result_in[...]
+    norm[...] = norm_in[...]
+    new_max[...] = max_in[...]
+    for n in range(pieces):
+        ins[n].wait()
+        for m in range(size):
+            s = n * size + m
+            for h in range(heads):
+                matrix[n, m, h] = forget[h, s] * state[n, m, h] + iv[h, :, s : s + 1] * kk[s, h : h + 1, :]
+        outs[n].start()
+    for copy in outs:
+        copy.wait()
 
 
 def layer_kernel(
@@ -89,6 +129,7 @@
     comb,
     zs2,
     zr2,
+    turn,
     local_sem,
     send_sem,
     recv_sem,
@@ -104,26 +145,29 @@
     c = lax.rem(t, 2)
     partner = {"tp": t + 1 - 2 * c}
     locals_ = []
+    early = 4
     for n, (src, dst) in enumerate(
         zip(
             (wq_hbm, wk_hbm, wv_hbm, wo_hbm, state_hbm, mix_hbm, sg_hbm, su_hbm, sd_hbm, eg_hbm, eu_hbm, ed_hbm),
             (wq, wk, wv, wo, state, mix, sg, su, sd, eg, eu, ed),
         )
     ):
-        copy = pltpu.make_async_copy(src, dst, local_sem.at[n])
+        locals_.append(pltpu.make_async_copy(src, dst, local_sem.at[n]))
+    for copy in locals_[:early]:
         copy.start()
-        locals_.append(copy)
 
     barrier = pltpu.get_barrier_semaphore()
     lo = rows // 16 * 16
     if lo < pad_rows:
         for buf in (rx_a, rx_b, ret_in):
-            buf[:, lo:, :] = jnp.zeros((E, pad_rows - lo, Z * SW), BF16)
+            buf[:, :, lo:, :] = jnp.zeros((Z, E, pad_rows - lo, SW), BF16)
+    ep_peers = partners(g, E)
+    z_peers = partners(z, Z)
     pl.semaphore_signal(barrier, inc=1, device_id=partner, device_id_type=MESH)
-    for d in range(1, Z):
-        pl.semaphore_signal(barrier, inc=1, device_id={"tp": lax.rem(z + d, Z) * 2 + c}, device_id_type=MESH)
-    for d in range(1, E):
-        pl.semaphore_signal(barrier, inc=1, device_id={"ep": lax.rem(g + d, E)}, device_id_type=MESH)
+    for to, _ in z_peers:
+        pl.semaphore_signal(barrier, inc=1, device_id={"tp": to * 2 + c}, device_id_type=MESH)
+    for to, _ in ep_peers:
+        pl.semaphore_signal(barrier, inc=1, device_id={"ep": to}, device_id_type=MESH)
 
     sent = []
 
@@ -141,18 +185,6 @@
         sent.append(copy)
         return copy
 
-    def ep_to(d):
-        return lax.rem(g + d, E)
-
-    def ep_from(d):
-        return lax.rem(g + E - d, E)
-
-    def z_to(d):
-        return lax.rem(z + d, Z)
-
-    def z_from(d):
-        return lax.rem(z + Z - d, Z)
-
     def columns(zi, core):
         return pl.ds(pl.multiple_of((zi * 2 + core) * SW, SW), SW)
 
@@ -167,8 +199,9 @@
         span = slice(p * Dk, (p + 1) * Dk)
         normed[p] = (hidden_ref[:, span].astype(F32) * scale * mix_gain_ref[:, span]).astype(BF16)
     pl.semaphore_wait(barrier, Z + E - 1)
-    moves = [remote(normed.at[ep_to(d)], gathered.at[g], {"ep": ep_to(d)}) for d in range(1, E)]
-    gathered[g] = normed[g]
+    moves = [remote(normed.at[to], gathered.at[g], {"ep": to}) for to, _ in ep_peers]
+    for copy in locals_[early:]:
+        copy.start()
 
     bias_t = transposed(0, bias_ref[...])
     gate_pre = []
@@ -220,19 +253,21 @@
 
     for n in range(4):
         locals_[n].wait()
-    for move in moves:
-        move.wait_recv()
-    stacked = gathered[...].reshape(E * S, Dk)
     hc = H * hd
-    for n, weight in enumerate((wq, wk, wv, wo)):
-        part[:, :, n * hc : (n + 1) * hc] = dot(stacked, weight[...]).astype(BF16).reshape(E, S, hc)
-    moves = [remote(part.at[ep_to(d)], proj_in.at[g], {"ep": ep_to(d)}) for d in range(1, E)]
+
+    def project(block):
+        return jnp.concatenate([dot(block, w[...]) for w in (wq, wk, wv, wo)], -1)
+
+    projected = project(normed[g])
+    back_moves = []
+    for move, (_, source) in zip(moves, ep_peers):
+        move.wait_recv()
+        part[source] = project(gathered[source]).astype(BF16)
+        back_moves.append(remote(part.at[source], proj_in.at[g], {"ep": source}))
     locals_[4].wait()
-    for move in moves:
-        move.wait_recv()
-    projected = part[g].astype(F32)
-    for d in range(1, E):
-        projected = projected + proj_in[ep_from(d)].astype(F32)
+    for move, (source, _) in zip(back_moves, ep_peers):
+        move.wait_recv()
+        projected = projected + proj_in[source].astype(F32)
     projected = projected.astype(BF16).astype(F32)
 
     for h in range(H):
@@ -258,7 +293,8 @@
         put_value = put * value
         new_norm = keep * norm_ref[:, h, :] + put * key
         new_norm_ref[:, h, :] = new_norm
-        iv_ref[:, h, :] = put_value
+        turn[:, :hd] = put_value
+        iv_ref[h] = turn[...].T[:hd, :]
         kk_ref[:, h, :] = key
         numerator = keep * reads[h].T[:S, :] + put_value * jnp.sum(key * query, -1, keepdims=True)
         denominator = jnp.maximum(jnp.abs(jnp.sum(new_norm * query, -1, keepdims=True)), 1.0)
@@ -266,39 +302,55 @@
     gated = jnp.concatenate(gated, -1).astype(BF16)
 
     locals_[5].wait()
+    far_first = z_peers[::-1]
+    chunks = [to for to, _ in far_first] + [z]
+    pair_moves = []
+    for to in chunks:
+        mix_out[to] = dot(gated, mix[:, columns(to, 1 - c)]).astype(BF16)
+        pair_moves.append(remote(mix_out.at[to], mix_in.at[to], partner))
     moves = []
-    for zi in range(Z):
-        mix_out[zi] = dot(gated, mix[:, columns(zi, 1 - c)]).astype(BF16)
-        moves.append(remote(mix_out.at[zi], mix_in.at[zi], partner))
-    for zi in range(Z):
-        mix_own[zi] = dot(gated, mix[:, columns(zi, c)])
-    for move in moves:
-        move.wait_recv()
-    moves = []
-    for d in range(1, Z):
-        to = z_to(d)
-        zs[to] = (mix_own[to] + mix_in[to].astype(F32)).astype(BF16)
-        moves.append(remote(zs.at[to], zr.at[z], {"tp": to * 2 + c}))
-    mixed = hidden_ref[:, columns(z, c)].astype(F32) + mix_own[z] + mix_in[z].astype(F32)
-    for d in range(1, Z):
-        moves[d - 1].wait_recv()
-        mixed = mixed + zr[z_from(d)].astype(F32)
+    for n, to in enumerate(chunks):
+        own = dot(gated, mix[:, columns(to, c)])
+        pair_moves[n].wait_recv()
+        own = own + mix_in[to].astype(F32)
+        if n < Z - 1:
+            zs[to] = own.astype(BF16)
+            moves.append(remote(zs.at[to], zr.at[z], {"tp": to * 2 + c}))
+        else:
+            mixed = own + hidden_ref[:, columns(z, c)].astype(F32)
+    for move, (_, source) in zip(moves, far_first):
+        move.wait_recv()
+        mixed = mixed + zr[source].astype(F32)
     stream_own = mixed.astype(BF16)
 
+    kept = pl.ds(0, -(-rows // 8) * 8)
+    row_moves = []
+    row_shares = []
+
+    def select(chunk):
+        sel[chunk] = dot(chooser, half[chunk]).astype(BF16).reshape(E, pad_rows, SW)
+        for to, source in ep_peers[::-1]:
+            move = remote(sel.at[chunk, to, kept], rx_a.at[chunk, g, kept], {"ep": to})
+            row_moves.append((move, chunk, source))
+        row_shares.append(remote(sel.at[chunk, g, kept], rx_b.at[chunk, g, kept], partner))
+        rx_a[chunk, g] = sel[chunk, g]
+
+    def hand_over(entries):
+        for move, chunk, source in entries:
+            move.wait_recv()
+            row_shares.append(
+                remote(rx_a.at[chunk, source, kept], rx_b.at[chunk, source, kept], partner)
+            )
+
     half[z] = stream_own
-    moves = [remote(half.at[z], half.at[z], {"tp": z_to(d) * 2 + c}) for d in range(1, Z)]
+    moves = [remote(half.at[z], half.at[z], {"tp": to * 2 + c}) for to, _ in far_first][::-1]
     shares = [remote(half.at[z], other.at[z], partner)]
-    for d in range(1, Z):
-        moves[d - 1].wait_recv()
-        shares.append(remote(half.at[z_from(d)], other.at[z_from(d)], partner))
-    for zi in range(Z):
-        sel[:, :, zi * SW : (zi + 1) * SW] = dot(chooser, half[zi]).astype(BF16).reshape(E, pad_rows, SW)
-    kept = pl.ds(0, -(-rows // 8) * 8)
-    moves = [
-        remote(sel.at[ep_to(d), kept], rx_a.at[g, kept], {"ep": ep_to(d)}) for d in range(1, E)
-    ]
-    rows_shares = [remote(sel.at[g, kept], rx_b.at[g, kept], partner)]
-    rx_a[g] = sel[g]
+    select(z)
+    for move, (_, source) in zip(moves, z_peers):
+        move.wait_recv()
+        shares.append(remote(half.at[source], other.at[source], partner))
+        select(source)
+    hand_over(row_moves[: 2 * (E - 1)])
 
     for move in shares:
         move.wait_recv()
@@ -317,6 +369,7 @@
     inputs = x_shared[...]
     gate = dot(inputs, sg[...])
     shared_hidden = (gate / (1.0 + jnp.exp(-gate)) * dot(inputs, su[...])).astype(BF16)
+    hand_over(row_moves[2 * (E - 1) :])
     shared_moves = []
     for zi in range(Z):
         sh_out[zi] = dot(shared_hidden, sd[:, columns(zi, 1 - c)]).astype(BF16)
@@ -324,22 +377,19 @@
     for zi in range(Z):
         sh_own[zi] = dot(shared_hidden, sd[:, columns(zi, c)])
 
-    for d in range(1, E):
-        moves[d - 1].wait_recv()
-        rows_shares.append(remote(rx_a.at[ep_from(d), kept], rx_b.at[ep_from(d), kept], partner))
-    for move in rows_shares:
+    for move in row_shares:
         move.wait_recv()
     count = E * pad_rows
     squares = jnp.zeros((count, 1), F32)
     for buf in (rx_a, rx_b):
         for zi in range(Z):
-            floats = buf[:, :, zi * SW : (zi + 1) * SW].reshape(count, SW).astype(F32)
+            floats = buf[zi].reshape(count, SW).astype(F32)
             squares = squares + jnp.sum(floats * floats, -1, keepdims=True)
     scale = lax.rsqrt(squares / D + norm_eps)
     for zi in range(Z):
         for buf, core in ((rx_a, c), (rx_b, 1 - c)):
             span = columns(zi, core)
-            floats = buf[:, :, zi * SW : (zi + 1) * SW].reshape(count, SW).astype(F32)
+            floats = buf[zi].reshape(count, SW).astype(F32)
             x_rows[:, span] = (floats * scale * ffn_gain_ref[:, span]).astype(BF16)
     for n in range(9, 12):
         locals_[n].wait()
@@ -351,37 +401,39 @@
         value = jnp.where((place >= e * cap) & (place < (e + 1) * cap), value, 0.0)
         hid[:, e * width : (e + 1) * width] = value.astype(BF16)
     pair_moves = []
-    for zi in range(Z):
-        pair_out[zi] = dot(hid[...], ed[:, columns(zi, 1 - c)]).astype(BF16)
-        pair_moves.append(remote(pair_out.at[zi], pair_in.at[zi], partner))
-    for zi in range(Z):
-        pair_own[zi] = dot(hid[...], ed[:, columns(zi, c)])
-    for zi in range(Z):
-        pair_moves[zi].wait_recv()
-        both = pair_own[zi] + pair_in[zi].astype(F32)
-        ret_out[:, :, zi * SW : (zi + 1) * SW] = both.astype(BF16).reshape(E, pad_rows, SW)
-    moves = [
-        remote(ret_out.at[ep_to(d), kept], ret_in.at[g, kept], {"ep": ep_to(d)})
-        for d in range(1, E)
-    ]
-    ret_in[g] = ret_out[g]
+    for to in chunks:
+        pair_out[to] = dot(hid[...], ed[:, columns(to, 1 - c)]).astype(BF16)
+        pair_moves.append(remote(pair_out.at[to], pair_in.at[to], partner))
+    ret_moves = []
+    for n, chunk in enumerate(chunks):
+        own = dot(hid[...], ed[:, columns(chunk, c)])
+        pair_moves[n].wait_recv()
+        both = own + pair_in[chunk].astype(F32)
+        ret_out[chunk] = both.astype(BF16).reshape(E, pad_rows, SW)
+        ret_moves.append(
+            [
+                remote(ret_out.at[chunk, to, kept], ret_in.at[chunk, g, kept], {"ep": to})
+                for to, _ in ep_peers[::-1]
+            ]
+        )
+        ret_in[chunk, g] = ret_out[chunk, g]
     for move in shared_moves:
         move.wait_recv()
-    for move in moves:
-        move.wait_recv()
-
-    for zi in range(Z):
-        back = ret_in[:, :, zi * SW : (zi + 1) * SW].reshape(count, SW)
-        comb[zi] = dot(share_hi, back) + dot(share_lo, back) + sh_own[zi] + sh_in[zi].astype(F32)
+
     moves = []
-    for d in range(1, Z):
-        to = z_to(d)
-        zs2[to] = comb[to].astype(BF16)
-        moves.append(remote(zs2.at[to], zr2.at[z], {"tp": to * 2 + c}))
-    total = half[z].astype(F32) + comb[z]
-    for d in range(1, Z):
-        moves[d - 1].wait_recv()
-        total = total + zr2[z_from(d)].astype(F32)
+    for n, chunk in enumerate(chunks):
+        for move in ret_moves[n]:
+            move.wait_recv()
+        back = ret_in[chunk].reshape(count, SW)
+        own = dot(share_hi, back) + dot(share_lo, back) + sh_own[chunk] + sh_in[chunk].astype(F32)
+        if n < Z - 1:
+            zs2[chunk] = own.astype(BF16)
+            moves.append(remote(zs2.at[chunk], zr2.at[z], {"tp": chunk * 2 + c}))
+        else:
+            total = half[z].astype(F32) + own
+    for move, (_, source) in zip(moves, far_first):
+        move.wait_recv()
+        total = total + zr2[source].astype(F32)
     result_ref[...] = total.astype(BF16)
     for copy in sent:
         copy.wait_send()
@@ -429,7 +481,7 @@
         shared_gate, shared_up, shared_down, expert_gate, expert_up, down,
     )
     V = pltpu.VMEM
-    sems = 6 * E + 8 * Z + 8
+    sems = (2 + 3 * Z) * E + 10 * Z + 8
     result, new_max, new_norm, forget, iv, kk = pl.pallas_call(
         functools.partial(layer_kernel, dims),
         out_shape=(
@@ -437,7 +489,7 @@
             jax.ShapeDtypeStruct((H, S), F32),
             jax.ShapeDtypeStruct((S, H, hd), F32),
             jax.ShapeDtypeStruct((H, S), F32),
-            jax.ShapeDtypeStruct((S, H, hd), F32),
+            jax.ShapeDtypeStruct((H, hd, S), F32),
             jax.ShapeDtypeStruct((S, H, hd), F32),
         ),
         in_specs=[vmem] * 9 + [hbm] * len(big),
@@ -458,9 +510,9 @@
             V((Z, S, SW), BF16),
             V((Z, S, SW), BF16),
             V((Z, S, SW), BF16),
-            V((E, pad_rows, Z * SW), BF16),
-            V((E, pad_rows, Z * SW), BF16),
-            V((E, pad_rows, Z * SW), BF16),
+            V((Z, E, pad_rows, SW), BF16),
+            V((Z, E, pad_rows, SW), BF16),
+            V((Z, E, pad_rows, SW), BF16),
             V((S, D), BF16),
             V((Z, S, SW), BF16),
             V((Z, S, SW), BF16),
@@ -470,11 +522,12 @@
             V((Z, count, SW), BF16),
             V((Z, count, SW), BF16),
             V((Z, count, SW), F32),
-            V((E, pad_rows, Z * SW), BF16),
-            V((E, pad_rows, Z * SW), BF16),
+            V((Z, E, pad_rows, SW), BF16),
+            V((Z, E, pad_rows, SW), BF16),
             V((Z, S, SW), F32),
             V((Z, S, SW), BF16),
             V((Z, S, SW), BF16),
+            V((S, 128), F32),
             pltpu.SemaphoreType.DMA((len(big),)),
             pltpu.SemaphoreType.DMA((sems,)),
             pltpu.SemaphoreType.DMA((sems,)),
@@ -495,7 +548,27 @@
         route_weights.T,
         *big,
     )
-    new_matrix = forget.T[:, :, None, None] * state_matrix + iv[..., :, None] * kk[..., None, :]
+    pieces = 4 if S % 4 == 0 else 1
+    held = (pieces, S // pieces, H, hd, hd)
+    result, new_matrix, new_norm, new_max = pl.pallas_call(
+        memory_kernel,
+        out_shape=(
+            jax.ShapeDtypeStruct((S, SW), BF16),
+            jax.ShapeDtypeStruct(state_matrix.shape, F32),
+            jax.ShapeDtypeStruct((S, H, hd), F32),
+            jax.ShapeDtypeStruct((H, S), F32),
+        ),
+        in_specs=[vmem] * 3 + [pl.BlockSpec(memory_space=pltpu.SMEM)] + [vmem] * 2 + [hbm],
+        out_specs=(vmem, hbm, vmem, vmem),
+        scratch_shapes=[
+            V(held, F32),
+            V(held, F32),
+            pltpu.SemaphoreType.DMA((pieces,)),
+            pltpu.SemaphoreType.DMA((pieces,)),
+        ],
+        compiler_params=pltpu.CompilerParams(vmem_limit_bytes=40 * 1024 * 1024),
+        name="memory",
+    )(result, new_norm, new_max, forget, iv, kk, state_matrix)
     return (result, new_matrix, new_norm, new_max.T)
 
 

time: 63.7 us -> 63.7 us (level)
  other arithmetic: 5.84 us -> 0 us
  local copies, waits for them, and re-layouts: 2.59 us -> 6.86 us
  Pallas kernels: 54.4 us -> 55.8 us
    add x1 -> x0, other arithmetic: 5.84 us -> none  [per_device(): forget.T[:, :, None, None] * state_matrix]
    unnamed x9 -> x14, local copies, waits for them, and re-layouts: 1.83 us -> 6.86 us
    pallas_call x0 -> x1, Pallas kernels: none -> 3.96 us  [per_device(): pl.pallas_call(memory_kernel, out_shape=(jax.ShapeDtypeStruct((S, SW), BF...]
    pallas_call x1, Pallas kernels: 54.4 us -> 51.8 us  [per_device(): pl.pallas_call(functools.partial(layer_kernel, dims), out_shape=(jax.Shap...]
    transpose x1 -> x0, local copies, waits for them, and re-layouts: 0.76 us -> none  [per_device(): forget.T[:, :, None, None] * state_matrix]
where the time goes in v2:
time: 63.7 us; the launch traced here: 63.3 us
  Pallas kernels  55.8 us (88%)
  local copies, waits for them, and re-layouts  6.86 us (11%)
  between operations  0.66 us (1%)
    pallas_call x1, Pallas kernels, per_device(): pl.pallas_call(functools.partial(layer_kernel, dims), out_shape=(jax.Shap...  51.8 us
    unnamed x14, local copies, waits for them, and re-layouts  6.86 us
    pallas_call x1, Pallas kernels, per_device(): pl.pallas_call(memory_kernel, out_shape=(jax.ShapeDtypeStruct((S, SW), BF...  3.96 us

profile of v2, /device:TPU:0, one launch (start us, length us, event | category | flops | bytes accessed | tf_op | source)
XLA Modules:
  0.0 63.3 jit_solution(14549792724814990327)
XLA Ops:
  0.6 51.8 %layer.1 = (bf16[32,512]{1,0:T(8,128)(2,1)}, f32[4,32]{1,0:T(4,128)}, f32[32,4,64]{2,1,0:T(4,128)}, f32[4,32]{1,0:T(4,128)}, f32[4,64,32]{2,1,0:T(8,128)}, /*index=5*/f32[32,4,64]{2,1,0:T(4,128)}) custom-call(bf16[32,4096]{1,0:T(8,128)(2,1)} %hidden_ref.1, f32[1,4096]{1,0:T(1,128)} %bitcast.10, bf16[2,4,4096]{2,1,0:T(4,128)(2,1)} %bitcast.9, ...), custom_call_target="tpu_custom_call" | custom-call | tf_op jit(solution)/shard_map/layer/pallas_call | solution.py:485
  52.5 0.0 copy-start
  52.5 2.2 %copy-done = f32[32,4,64,64]{3,2,1,0:T(8,128)S(1)} copy-done((f32[32,4,64,64]{3,2,1,0:T(8,128)S(1)}, f32[32,4,64,64]{3,2,1,0:T(8,128)}, u32[]{:S(2)}) %copy-start) | copy-done | bytes 2097176
  54.7 0.0 copy-start.1
  54.7 0.9 %copy-done.1 = f32[4,64,32]{2,1,0:T(8,128)S(1)} copy-done((f32[4,64,32]{2,1,0:T(8,128)S(1)}, f32[4,64,32]{2,1,0:T(8,128)}, u32[]{:S(2)}) %copy-start.1) | copy-done | bytes 32792
  55.6 0.0 copy-start.2
  55.6 0.8 %copy-done.2 = f32[32,4,64]{2,1,0:T(4,128)S(1)} copy-done((f32[32,4,64]{2,1,0:T(4,128)S(1)}, f32[32,4,64]{2,1,0:T(4,128)}, u32[]{:S(2)}) %copy-start.2) | copy-done | bytes 32792
  56.4 0.0 copy-start.3
  56.4 0.8 %copy-done.3 = f32[32,4,64]{2,1,0:T(4,128)S(1)} copy-done((f32[32,4,64]{2,1,0:T(4,128)S(1)}, f32[32,4,64]{2,1,0:T(4,128)}, u32[]{:S(2)}) %copy-start.3) | copy-done | bytes 32792
  57.3 0.0 copy-start.4
  57.3 0.8 %copy-done.4 = bf16[32,512]{1,0:T(8,128)(2,1)S(1)} copy-done((bf16[32,512]{1,0:T(8,128)(2,1)S(1)}, bf16[32,512]{1,0:T(8,128)(2,1)}, u32[]{:S(2)}) %copy-start.4) | copy-done | bytes 32792
  58.0 0.0 copy-start.5
  58.0 0.7 %copy-done.5 = f32[4,32]{1,0:T(4,128)S(1)} copy-done((f32[4,32]{1,0:T(4,128)S(1)}, f32[4,32]{1,0:T(4,128)}, u32[]{:S(2)}) %copy-start.5) | copy-done | bytes 536
  58.7 0.0 copy-start.6
  58.7 0.7 %copy-done.6 = f32[4,32]{1,0:T(4,128)S(1)} copy-done((f32[4,32]{1,0:T(4,128)S(1)}, f32[4,32]{1,0:T(4,128)}, u32[]{:S(2)}) %copy-start.6) | copy-done | bytes 536
  59.4 4.0 %memory.1 = (bf16[32,512]{1,0:T(8,128)(2,1)}, f32[32,4,64,64]{3,2,1,0:T(8,128)}, f32[32,4,64]{2,1,0:T(4,128)}, f32[4,32]{1,0:T(4,128)}) custom-call(bf16[32,512]{1,0:T(8,128)(2,1)S(1)} %copy-done.4, f32[32,4,64]{2,1,0:T(4,128)S(1)} %copy-done.2, f32[4,32]{1,0:T(4,128)S(1)} %copy-done.5, f32[4,32]{1,0:T(4,128)S(1)} %copy-done.6, f32[4,64,32]{2,1,0:T(8,128)S(1)} %copy-done.1, ...), custom_call_target="tpu_custom_call" | custom-call | tf_op jit(solution)/shard_map/memory/pallas_call | solution.py:553
Async XLA Ops:
  52.5 2.2 %copy-start = (f32[32,4,64,64]{3,2,1,0:T(8,128)S(1)}, f32[32,4,64,64]{3,2,1,0:T(8,128)}, u32[]{:S(2)}) copy-start(f32[32,4,64,64]{3,2,1,0:T(8,128)} %state_hbm.3) | copy-start | bytes 6291460
  54.7 0.9 %copy-start.1 = (f32[4,64,32]{2,1,0:T(8,128)S(1)}, f32[4,64,32]{2,1,0:T(8,128)}, u32[]{:S(2)}) copy-start(f32[4,64,32]{2,1,0:T(8,128)} %get-tuple-element.18.iv) | copy-start | bytes 98308
  55.6 0.8 %copy-start.2 = (f32[32,4,64]{2,1,0:T(4,128)S(1)}, f32[32,4,64]{2,1,0:T(4,128)}, u32[]{:S(2)}) copy-start(f32[32,4,64]{2,1,0:T(4,128)} %get-tuple-element.15.norm_in) | copy-start | bytes 98308
  56.4 0.8 %copy-start.3 = (f32[32,4,64]{2,1,0:T(4,128)S(1)}, f32[32,4,64]{2,1,0:T(4,128)}, u32[]{:S(2)}) copy-start(f32[32,4,64]{2,1,0:T(4,128)} %get-tuple-element.19.kk) | copy-start | bytes 98308
  57.3 0.8 %copy-start.4 = (bf16[32,512]{1,0:T(8,128)(2,1)S(1)}, bf16[32,512]{1,0:T(8,128)(2,1)}, u32[]{:S(2)}) copy-start(bf16[32,512]{1,0:T(8,128)(2,1)} %get-tuple-element.14.result_in) | copy-start | bytes 98308
  58.0 0.7 %copy-start.5 = (f32[4,32]{1,0:T(4,128)S(1)}, f32[4,32]{1,0:T(4,128)}, u32[]{:S(2)}) copy-start(f32[4,32]{1,0:T(4,128)} %get-tuple-element.16.max_in) | copy-start | bytes 1540
  58.7 0.7 %copy-start.6 = (f32[4,32]{1,0:T(4,128)S(1)}, f32[4,32]{1,0:T(4,128)}, u32[]{:S(2)}) copy-start(f32[4,32]{1,0:T(4,128)} %get-tuple-element.17.forget) | copy-start | bytes 1540

commit v3 on v2

--- a/solution.py
+++ b/solution.py
@@ -352,30 +352,7 @@
         select(source)
     hand_over(row_moves[: 2 * (E - 1)])
 
-    for move in shares:
-        move.wait_recv()
-    squares = jnp.zeros((S, 1), F32)
-    for zi in range(Z):
-        for buf in (half, other):
-            floats = buf[zi].astype(F32)
-            squares = squares + jnp.sum(floats * floats, -1, keepdims=True)
-    scale = lax.rsqrt(squares / D + norm_eps)
-    for zi in range(Z):
-        for buf, core in ((half, c), (other, 1 - c)):
-            span = columns(zi, core)
-            x_shared[:, span] = (buf[zi].astype(F32) * scale * ffn_gain_ref[:, span]).astype(BF16)
-    for n in range(6, 9):
-        locals_[n].wait()
-    inputs = x_shared[...]
-    gate = dot(inputs, sg[...])
-    shared_hidden = (gate / (1.0 + jnp.exp(-gate)) * dot(inputs, su[...])).astype(BF16)
     hand_over(row_moves[2 * (E - 1) :])
-    shared_moves = []
-    for zi in range(Z):
-        sh_out[zi] = dot(shared_hidden, sd[:, columns(zi, 1 - c)]).astype(BF16)
-        shared_moves.append(remote(sh_out.at[zi], sh_in.at[zi], partner))
-    for zi in range(Z):
-        sh_own[zi] = dot(shared_hidden, sd[:, columns(zi, c)])
 
     for move in row_shares:
         move.wait_recv()
@@ -417,6 +394,30 @@
             ]
         )
         ret_in[chunk, g] = ret_out[chunk, g]
+
+    for move in shares:
+        move.wait_recv()
+    squares = jnp.zeros((S, 1), F32)
+    for zi in range(Z):
+        for buf in (half, other):
+            floats = buf[zi].astype(F32)
+            squares = squares + jnp.sum(floats * floats, -1, keepdims=True)
+    scale = lax.rsqrt(squares / D + norm_eps)
+    for zi in range(Z):
+        for buf, core in ((half, c), (other, 1 - c)):
+            span = columns(zi, core)
+            x_shared[:, span] = (buf[zi].astype(F32) * scale * ffn_gain_ref[:, span]).astype(BF16)
+    for n in range(6, 9):
+        locals_[n].wait()
+    inputs = x_shared[...]
+    gate = dot(inputs, sg[...])
+    shared_hidden = (gate / (1.0 + jnp.exp(-gate)) * dot(inputs, su[...])).astype(BF16)
+    shared_moves = []
+    for zi in range(Z):
+        sh_out[zi] = dot(shared_hidden, sd[:, columns(zi, 1 - c)]).astype(BF16)
+        shared_moves.append(remote(sh_out.at[zi], sh_in.at[zi], partner))
+    for zi in range(Z):
+        sh_own[zi] = dot(shared_hidden, sd[:, columns(zi, c)])
     for move in shared_moves:
         move.wait_recv()
 
@@ -566,7 +567,7 @@
             pltpu.SemaphoreType.DMA((pieces,)),
             pltpu.SemaphoreType.DMA((pieces,)),
         ],
-        compiler_params=pltpu.CompilerParams(vmem_limit_bytes=40 * 1024 * 1024),
+        compiler_params=pltpu.CompilerParams(vmem_limit_bytes=60 * 1024 * 1024),
         name="memory",
     )(result, new_norm, new_max, forget, iv, kk, state_matrix)
     return (result, new_matrix, new_norm, new_max.T)

time: 63.7 us -> 58 us (0.911)
  local copies, waits for them, and re-layouts: 6.86 us -> 0 us
  Pallas kernels: 55.8 us -> 57.2 us
    unnamed x14 -> x0, local copies, waits for them, and re-layouts: 6.86 us -> none
    pallas_call x1, Pallas kernels: 3.96 us -> 5.27 us  [per_device(): pl.pallas_call(memory_kernel, out_shape=(jax.ShapeDtypeStruct((S, SW), BF...]
where the time goes in v3:
time: 58 us; the launch traced here: 57.9 us
  Pallas kernels  57.2 us (99%)
  between operations  0.65 us (1%)
    pallas_call x1, Pallas kernels, per_device(): pl.pallas_call(functools.partial(layer_kernel, dims), out_shape=(jax.Shap...  52 us
    pallas_call x1, Pallas kernels, per_device(): pl.pallas_call(memory_kernel, out_shape=(jax.ShapeDtypeStruct((S, SW), BF...  5.27 us

profile of v3, /device:TPU:0, one launch (start us, length us, event | category | flops | bytes accessed | tf_op | source)
XLA Modules:
  0.0 57.9 jit_solution(1265237025468540726)
XLA Ops:
  0.6 52.0 %layer.1 = (bf16[32,512]{1,0:T(8,128)(2,1)}, f32[4,32]{1,0:T(4,128)}, f32[32,4,64]{2,1,0:T(4,128)}, f32[4,32]{1,0:T(4,128)}, f32[4,64,32]{2,1,0:T(8,128)}, /*index=5*/f32[32,4,64]{2,1,0:T(4,128)}) custom-call(bf16[32,4096]{1,0:T(8,128)(2,1)} %hidden_ref.1, f32[1,4096]{1,0:T(1,128)} %bitcast.10, bf16[2,4,4096]{2,1,0:T(4,128)(2,1)} %bitcast.9, ...), custom_call_target="tpu_custom_call" | custom-call | tf_op jit(solution)/shard_map/layer/pallas_call | solution.py:486
  52.6 5.3 %memory.1 = (bf16[32,512]{1,0:T(8,128)(2,1)}, f32[32,4,64,64]{3,2,1,0:T(8,128)}, f32[32,4,64]{2,1,0:T(4,128)}, f32[4,32]{1,0:T(4,128)}) custom-call(bf16[32,512]{1,0:T(8,128)(2,1)} %get-tuple-element.14.result_in, f32[32,4,64]{2,1,0:T(4,128)} %get-tuple-element.15.norm_in, f32[4,32]{1,0:T(4,128)} %get-tuple-element.16.max_in, ...), custom_call_target="tpu_custom_call" | custom-call | tf_op jit(solution)/shard_map/memory/pallas_call | solution.py:554
